TPU v7x, 32 devices: a whole 2x2x4 slice. The times are simulated.
32 devices in a mesh: ep: 8 (over z, y), tp: 4 (over x, core).
Axes of the slice: x: 2, y: 2, z: 4, core: 2. Of those that a mesh axis runs over, the one named last changes fastest.
Arguments:
- tokens: bfloat16 [2048, 2048], P('ep', 'tp'), may hold values from -400 to 400
- expert_ids: int32 [2048, 2], P('ep'), may hold values from 0 to 7, all different within a row; in each aligned block of 256 rows (0 to 255, 256 to 511, ...) at most 80 rows name the same one
- route_weights: float32 [2048, 2], P('ep'), may hold values from 0.1 to 1
- pre_gain: float32 [2048], P('tp'), may hold values from 0.1 to 1.9
- post_gain: float32 [2048], P('tp'), may hold values from 0.1 to 1.9
- gate_weight: bfloat16 [8, 2048, 4096], P('ep', None, 'tp'), may hold values from -0.125 to 0.125
- up_weight: bfloat16 [8, 2048, 4096], P('ep', None, 'tp'), may hold values from -0.125 to 0.125
- down_weight: bfloat16 [8, 4096, 2048], P('ep', None, 'tp'), may hold values from -0.71875 to 0.71875
Outputs:
- layer_out: bfloat16 [2048, 2048], P('ep', 'tp')
Inputs may be any that keep to these rules, and one draw needn't show every extreme that they name: `expert_ids`: the 2 experts of a token are distinct. Within the rows of one device along ep, no expert is named more than 80 times, a bound that some block reaches.
All inputs are finite; a program needn't handle non-finite values.
Results may differ from a plain program's by a relative error of at most 0.007.
Values may be sent and summed in bfloat16 or wider, within the bound.
A program may use at most 64 MiB of HBM per device.

v0:
```python
import jax
import jax.numpy as jnp
from jax import lax
from jax.sharding import PartitionSpec as P

epsilon = 1e-06


def on_device(
    tokens, expert_ids, route_weights, pre_gain, post_gain, gate_weight, up_weight, down_weight
):
    tok_rows, width_part = tokens.shape
    width_full = width_part * lax.axis_size("tp")
    ep_count = lax.axis_size("ep")
    local_count = gate_weight.shape[0]
    experts_all = local_count * ep_count
    top_count = expert_ids.shape[1]
    capacity = max(2, tok_rows * top_count * 5 // (4 * experts_all))
    slot_total = experts_all * capacity
    tok_float = tokens.astype(jnp.float32)
    square_sum = lax.psum(jnp.sum(tok_float * tok_float, axis=1), "tp")
    inv_scale = lax.rsqrt(square_sum / width_full + epsilon)
    normed = (tok_float * inv_scale[:, None] * pre_gain[None, :]).astype(jnp.bfloat16)
    flat_ids = expert_ids.reshape(-1)
    onehot = (flat_ids[:, None] == jnp.arange(experts_all, dtype=jnp.int32)[None, :]).astype(
        jnp.int32
    )
    slot = jnp.sum((jnp.cumsum(onehot, axis=0) - 1) * onehot, axis=1)
    target = (flat_ids * capacity + slot).reshape(tok_rows, top_count)
    slot_index = jnp.arange(slot_total, dtype=jnp.int32)
    pick_map = (jnp.transpose(target).reshape(-1)[:, None] == slot_index[None, :]).astype(
        jnp.bfloat16
    )
    dispatch_map = jnp.sum(pick_map.reshape(top_count, tok_rows, slot_total), axis=0)
    outgoing = jnp.dot(
        jnp.transpose(dispatch_map), normed, preferred_element_type=jnp.float32
    ).astype(jnp.bfloat16)
    outgoing = outgoing.reshape(ep_count, local_count, capacity, width_part)
    arrived = lax.all_to_all(outgoing, "ep", split_axis=0, concat_axis=2, tiled=True)
    arrived = arrived.reshape(local_count, ep_count * capacity, width_part)
    row_total = ep_count * capacity
    features = lax.all_gather(arrived, "tp", axis=2, tiled=True)
    gate = jnp.einsum("erd,edh->erh", features, gate_weight, preferred_element_type=jnp.float32)
    upper = jnp.einsum("erd,edh->erh", features, up_weight, preferred_element_type=jnp.float32)
    hidden = (jax.nn.silu(gate) * upper).astype(jnp.bfloat16)
    hidden_whole = lax.all_gather(hidden, "tp", axis=2, tiled=True)
    result = jnp.einsum(
        "erh,ehd->erd", hidden_whole, down_weight, preferred_element_type=jnp.float32
    )
    expert_out = result.astype(jnp.bfloat16).reshape(1, local_count, row_total, width_part)
    returned = lax.all_to_all(expert_out, "ep", split_axis=2, concat_axis=0, tiled=True)
    returned = returned.reshape(slot_total, width_part)
    picked = jnp.dot(pick_map, returned, preferred_element_type=jnp.float32).reshape(
        top_count, tok_rows, width_part
    )
    mixed = jnp.sum(picked * jnp.transpose(route_weights)[:, :, None], axis=0)
    out_sum = lax.psum(jnp.sum(mixed * mixed, axis=1), "tp")
    out_scale = lax.rsqrt(out_sum / width_full + epsilon)
    return (mixed * out_scale[:, None] * post_gain[None, :]).astype(jnp.bfloat16)


def solution(mesh):
    return jax.shard_map(
        on_device,
        mesh=mesh,
        in_specs=(
            P("ep", "tp"),
            P("ep", None),
            P("ep", None),
            P("tp"),
            P("tp"),
            P("ep", None, "tp"),
            P("ep", None, "tp"),
            P("ep", None, "tp"),
        ),
        out_specs=P("ep", "tp"),
        check_vma=False,
    )
```

profile of v0, /device:TPU:0, one launch (start us, length us, event | category | flops | bytes accessed | tf_op | source)
XLA Modules:
  0.0 170.0 jit_solution(17323781832735627482)
XLA Ops:
  6.5 0.0 all-gather.4.cloned.1.call-start
  6.5 0.8 copy.39
  7.4 0.1 eq.65
  7.5 0.1 eq.61
  7.7 1.1 reduce-window.6
  8.8 0.2 slice_reduce_fusion
  9.1 0.1 fusion.34
  9.2 0.1 reduce_sum.51
  9.3 0.1 copy.41
  9.4 0.7 add_bitcast_fusion
  10.1 0.2 fusion.24
  10.3 1.1 fusion.28
  11.4 8.4 %psum.14 = f32[256]{0:T(256)S(1)} all-reduce(f32[256]{0:T(256)S(1)} %fusion.28), channel_id=1, replica_groups=mesh['ep'=8,'tp'=4] {'tp'}, use_global_device_ids=true, to_apply=%region_5.6 | all-reduce | flops 256 | bytes 2048 | tf_op jit(solution)/shard_map/psum | solution.py:21
  19.7 1.4 convolution_convert_fusion
  21.1 22.2 %all_to_all.8 = bf16[8,1,80,512]{3,2,1,0:T(8,128)(2,1)} all-to-all(bf16[8,1,80,512]{3,2,1,0:T(8,128)(2,1)S(1)} %bitcast.53), channel_id=1, replica_groups=mesh['ep'=8,'tp'=4] {'ep'}, dimensions={0} | all-to-all | bytes 1310720 | tf_op jit(solution)/shard_map/all_to_all | solution.py:39
  43.3 0.0 all-gather.4.cloned.1.call-update
  43.4 0.0 all-gather.6.cloned.1.call-start
  43.4 24.3 %all-gather.4.cloned.1.call-done = bf16[1,640,2048]{2,1,0:T(8,128)(2,1)} async-done(((bf16[1,640,512]{2,1,0:T(8,128)(2,1)}), bf16[1,640,2048]{2,1,0:T(8,128)(2,1)}) %all-gather.4.cloned.1.call-update) | async-done | bytes 2621456 | tf_op jit(solution)/shard_map/all_gather | solution.py:42
  67.8 0.0 copy-start.1
  67.8 0.0 copy-start.2
  67.8 5.6 %fusion.4 = f32[640,1024]{1,0:T(8,128)S(1)} fusion(bf16[1,2048,1024]{2,1,0:T(8,128)(2,1)} %param.13, bf16[1,640,2048]{2,1,0:T(8,128)(2,1)} %all-gather.4.cloned.1.call-done), kind=kOutput, calls=%fused_computation.4 | convolution fusion | flops 2684354560 | bytes 9437184 | tf_op jit(solution)/shard_map/erd,edh->erh/dot_general | solution.py:43
  73.4 0.0 copy-done.1
  73.4 0.0 copy-done.2
  73.4 4.2 %multiply_convert_fusion = bf16[640,1024]{1,0:T(8,128)(2,1)} fusion(f32[640,1024]{1,0:T(8,128)S(1)} %fusion.4, bf16[1,2048,1024]{2,1,0:T(8,128)(2,1)S(1)} %copy-done.1, bf16[1,640,2048]{2,1,0:T(8,128)(2,1)S(1)} %copy-done.2), kind=kOutput, calls=%fused_computation.8 | convolution fusion | flops 2688286720 | bytes 10747904 | tf_op jit(solution)/shard_map/erd,edh->erh/dot_general | solution.py:44
  77.6 0.0 all-gather.6.cloned.1.call-update
  77.6 40.6 %all-gather.6.cloned.1.call-done = bf16[640,4096]{1,0:T(8,128)(2,1)} async-done(((bf16[640,1024]{1,0:T(8,128)(2,1)}), bf16[640,4096]{1,0:T(8,128)(2,1)}) %all-gather.6.cloned.1.call-update) | async-done | bytes 5242896 | tf_op jit(solution)/shard_map/all_gather | solution.py:46
  118.2 6.6 %fusion.21 = bf16[1,1,640,512]{3,2,1,0:T(8,128)(2,1)S(1)} fusion(bf16[640,4096]{1,0:T(8,128)(2,1)} %all-gather.6.cloned.1.call-done, bf16[1,4096,512]{2,1,0:T(8,128)(2,1)} %param.15), kind=kOutput, calls=%fused_computation.17 | convolution fusion | flops 2684682240 | bytes 10092544 | tf_op jit(solution)/shard_map/erh,ehd->erd/dot_general | solution.py:47
  124.8 1.0 copy.50
  125.8 0.5 broadcast.77
  126.3 4.8 %reduce.3 = bf16[640,512]{1,0:T(8,128)(2,1)S(1)} reduce(bf16[640,1,1,512]{3,2,1,0:T(2,128)(2,1)S(1)} %bitcast.51, bf16[]{:T(256)} %broadcast.77), dimensions={1,2}, to_apply=%bitcast.50.reduce_sub_computation | reduce | bytes 1310722
  131.1 0.0 copy-start.3
  131.1 0.5 reshape.125
  131.6 23.4 %all_to_all.9 = bf16[8,2,20480]{2,1,0:T(2,128)(2,1)S(1)} all-to-all(bf16[8,2,20480]{2,1,0:T(2,128)(2,1)S(1)} %reshape.125), channel_id=1, replica_groups=mesh['ep'=8,'tp'=4] {'ep'}, dimensions={0} | all-to-all | bytes 1310720 | tf_op jit(solution)/shard_map/all_to_all | solution.py:51
  155.0 0.0 copy-start
  155.0 0.6 reshape.126
  155.6 0.0 copy-done.3
  155.6 0.6 fusion.18
  156.3 0.1 multiply_reduce_fusion
  156.4 6.0 %psum.15 = f32[256]{0:T(256)S(1)} all-reduce(f32[256]{0:T(256)S(1)} %multiply_reduce_fusion), channel_id=1, replica_groups=mesh['ep'=8,'tp'=4] {'tp'}, use_global_device_ids=true, to_apply=%region_8.9 | all-reduce | flops 256 | bytes 2048 | tf_op jit(solution)/shard_map/psum | solution.py:57
  162.4 0.0 copy-done
  162.4 0.8 multiply_convert_fusion.1
  (5 shorter events, 0.1 us)
Async XLA Ops:
  6.5 61.2 %all-gather.4.cloned.1.call-start = ((), (), s32[]{:S(2)}) async-start(), calls=%async_computation.2 | async-start | bytes 3276800 | tf_op jit(solution)/shard_map/all_gather | solution.py:42
  43.4 74.8 %all-gather.6.cloned.1.call-start = ((), (), s32[]{:S(2)}) async-start(), calls=%async_computation.3 | async-start | bytes 6553600 | tf_op jit(solution)/shard_map/all_gather | solution.py:46
  67.8 5.6 %copy-start.1 = (bf16[1,2048,1024]{2,1,0:T(8,128)(2,1)S(1)}, bf16[1,2048,1024]{2,1,0:T(8,128)(2,1)}, u32[]{:S(2)}) copy-start(bf16[1,2048,1024]{2,1,0:T(8,128)(2,1)} %param.14) | copy-start | bytes 12582916
  67.8 5.6 %copy-start.2 = (bf16[1,640,2048]{2,1,0:T(8,128)(2,1)S(1)}, bf16[1,640,2048]{2,1,0:T(8,128)(2,1)}, u32[]{:S(2)}) copy-start(bf16[1,640,2048]{2,1,0:T(8,128)(2,1)} %all-gather.4.cloned.1.call-done) | copy-start | bytes 7864324
  131.1 24.5 %copy-start.3 = (f32[256,2]{0,1:T(2,128)S(1)}, f32[256,2]{0,1:T(2,128)}, u32[]{:S(2)}) copy-start(f32[256,2]{0,1:T(2,128)} %param.10) | copy-start | bytes 6148
  155.0 7.4 %copy-start = (f32[512]{0:T(512)S(1)}, f32[512]{0:T(512)}, u32[]{:S(2)}) copy-start(f32[512]{0:T(512)} %param.12) | copy-start | bytes 6148
Sparse Core Ops, SparseCore 0:
  43.5 24.2 all-gather.3
  77.7 40.3 all-gather.5
where the time goes:
time: 170 us
  waiting for transfers between devices  64.9 us (38%)
  blocking collectives  59.9 us (35%)
  matrix products  18.4 us (11%)
  between operations  13.5 us (8%)
  other arithmetic  8.99 us (5%)
  local copies, waits for them, and re-layouts  4.19 us (2%)
    all_gather x1, waiting for transfers between devices, on_device(): hidden_whole = lax.all_gather(hidden, 'tp', axis=2, tiled=True)  40.6 us
    all_gather x1, waiting for transfers between devices, on_device(): features = lax.all_gather(arrived, 'tp', axis=2, tiled=True)  24.3 us
    all_to_all x1, blocking collectives, on_device(): lax.all_to_all(expert_out, 'ep', split_axis=2, concat_axis=0, tiled=True)  23.4 us
    all_to_all x1, blocking collectives, on_device(): lax.all_to_all(outgoing, 'ep', split_axis=0, concat_axis=2, tiled=True)  22.2 us
    psum x1, blocking collectives, on_device(): square_sum = lax.psum(jnp.sum(tok_float * tok_float, axis=1), 'tp')  8.37 us
    dot_general x1, matrix products, on_device(): jnp.einsum('erh,ehd->erd', hidden_whole, down_weight, preferred_element_t...  6.62 us
    psum x1, blocking collectives, on_device(): out_sum = lax.psum(jnp.sum(mixed * mixed, axis=1), 'tp')  5.95 us
    dot_general x1, matrix products, on_device(): jnp.einsum('erd,edh->erh', features, gate_weight, preferred_element_type=...  5.58 us
  transfers between devices with their start and end apart: 2, of which 2 were waited for; matrix products, arithmetic and copies ran while one was open for 0% of the time, Pallas kernels for 0%

commit v1 on v0

--- a/solution.py
+++ b/solution.py
@@ -1,9 +1,25 @@
+import functools
 import jax
 import jax.numpy as jnp
 from jax import lax
 from jax.sharding import PartitionSpec as P
 
 epsilon = 1e-06
+
+
+def pass_the_values(local_values, shard_axis):
+    return jnp.concatenate(
+        jax.lax.all_to_all(
+            jnp.stack(jnp.split(local_values, jax.lax.axis_size(shard_axis), axis=2)),
+            shard_axis,
+            0,
+            0,
+        ),
+        axis=0,
+    )
+
+
+remake_row = functools.partial(pass_the_values, shard_axis="ep")
 
 
 def on_device(
@@ -48,7 +64,7 @@
         "erh,ehd->erd", hidden_whole, down_weight, preferred_element_type=jnp.float32
     )
     expert_out = result.astype(jnp.bfloat16).reshape(1, local_count, row_total, width_part)
-    returned = lax.all_to_all(expert_out, "ep", split_axis=2, concat_axis=0, tiled=True)
+    returned = remake_row(expert_out)
     returned = returned.reshape(slot_total, width_part)
     picked = jnp.dot(pick_map, returned, preferred_element_type=jnp.float32).reshape(
         top_count, tok_rows, width_part

time: 170 us -> 163 us (0.959)
  other arithmetic: 8.99 us -> 4.19 us
  local copies, waits for them, and re-layouts: 4.19 us -> 1.61 us
    unnamed x1 -> x0, other arithmetic: 4.79 us -> none
where the time goes in v1:
time: 163 us
  waiting for transfers between devices  64.9 us (40%)
  blocking collectives  59.9 us (37%)
  matrix products  18.4 us (11%)
  between operations  13.6 us (8%)
  other arithmetic  4.19 us (3%)
    all_gather x1, waiting for transfers between devices, on_device(): hidden_whole = lax.all_gather(hidden, 'tp', axis=2, tiled=True)  40.6 us
    all_gather x1, waiting for transfers between devices, on_device(): features = lax.all_gather(arrived, 'tp', axis=2, tiled=True)  24.3 us
    all_to_all x1, blocking collectives, pass_the_values(): jax.lax.all_to_all(jnp.stack(jnp.split(local_values, jax.lax.axis_size(sh...  23.4 us
    all_to_all x1, blocking collectives, on_device(): lax.all_to_all(outgoing, 'ep', split_axis=0, concat_axis=2, tiled=True)  22.2 us
    psum x1, blocking collectives, on_device(): square_sum = lax.psum(jnp.sum(tok_float * tok_float, axis=1), 'tp')  8.37 us
    dot_general x1, matrix products, on_device(): jnp.einsum('erh,ehd->erd', hidden_whole, down_weight, preferred_element_t...  6.62 us
    psum x1, blocking collectives, on_device(): out_sum = lax.psum(jnp.sum(mixed * mixed, axis=1), 'tp')  5.95 us
    dot_general x1, matrix products, on_device(): jnp.einsum('erd,edh->erh', features, gate_weight, preferred_element_type=...  5.58 us
  transfers between devices with their start and end apart: 2, of which 2 were waited for; matrix products, arithmetic and copies ran while one was open for 0% of the time, Pallas kernels for 0%

profile of v1, /device:TPU:0, one launch (start us, length us, event | category | flops | bytes accessed | tf_op | source)
XLA Modules:
  0.0 162.7 jit_solution(2785877836308564739)
XLA Ops:
  6.5 0.0 all-gather.4.cloned.1.call-start
  6.5 0.8 copy.29
  7.4 0.1 eq.65
  7.5 0.1 eq.61
  7.6 1.1 fusion.26
  8.7 8.4 %psum.14 = f32[256]{0:T(256)S(1)} all-reduce(f32[256]{0:T(256)S(1)} %fusion.26), channel_id=1, replica_groups=mesh['ep'=8,'tp'=4] {'tp'}, use_global_device_ids=true, to_apply=%region_5.6 | all-reduce | flops 256 | bytes 2048 | tf_op jit(solution)/shard_map/psum | solution.py:37
  17.1 1.1 reduce-window.6
  18.3 0.2 slice_reduce_fusion
  18.5 0.1 fusion.40
  18.6 0.1 reduce_sum.51
  18.8 0.1 copy.31
  18.8 0.7 add_bitcast_fusion
  19.5 0.2 fusion.24
  19.7 1.4 convolution_convert_fusion
  21.1 22.2 %all_to_all.14 = bf16[8,1,80,512]{3,2,1,0:T(8,128)(2,1)} all-to-all(bf16[8,1,80,512]{3,2,1,0:T(8,128)(2,1)S(1)} %bitcast.81), channel_id=1, replica_groups=mesh['ep'=8,'tp'=4] {'ep'}, dimensions={0} | all-to-all | bytes 1310720 | tf_op jit(solution)/shard_map/all_to_all | solution.py:55
  43.3 0.0 all-gather.4.cloned.1.call-update
  43.3 0.0 all-gather.6.cloned.1.call-start
  43.4 24.3 %all-gather.4.cloned.1.call-done = bf16[1,640,2048]{2,1,0:T(8,128)(2,1)} async-done(((bf16[1,640,512]{2,1,0:T(8,128)(2,1)}), bf16[1,640,2048]{2,1,0:T(8,128)(2,1)}) %all-gather.4.cloned.1.call-update) | async-done | bytes 2621456 | tf_op jit(solution)/shard_map/all_gather | solution.py:58
  67.7 0.0 copy-start.1
  67.7 0.0 copy-start.2
  67.7 5.6 %fusion.4 = f32[640,1024]{1,0:T(8,128)S(1)} fusion(bf16[1,2048,1024]{2,1,0:T(8,128)(2,1)} %param.13, bf16[1,640,2048]{2,1,0:T(8,128)(2,1)} %all-gather.4.cloned.1.call-done), kind=kOutput, calls=%fused_computation.4 | convolution fusion | flops 2684354560 | bytes 9437184 | tf_op jit(solution)/shard_map/erd,edh->erh/dot_general | solution.py:59
  73.3 0.0 copy-done.1
  73.4 0.0 copy-done.2
  73.4 4.2 %multiply_convert_fusion = bf16[640,1024]{1,0:T(8,128)(2,1)} fusion(f32[640,1024]{1,0:T(8,128)S(1)} %fusion.4, bf16[1,2048,1024]{2,1,0:T(8,128)(2,1)S(1)} %copy-done.1, bf16[1,640,2048]{2,1,0:T(8,128)(2,1)S(1)} %copy-done.2), kind=kOutput, calls=%fused_computation.8 | convolution fusion | flops 2688286720 | bytes 10747904 | tf_op jit(solution)/shard_map/erd,edh->erh/dot_general | solution.py:60
  77.6 0.0 all-gather.6.cloned.1.call-update
  77.6 40.6 %all-gather.6.cloned.1.call-done = bf16[640,4096]{1,0:T(8,128)(2,1)} async-done(((bf16[640,1024]{1,0:T(8,128)(2,1)}), bf16[640,4096]{1,0:T(8,128)(2,1)}) %all-gather.6.cloned.1.call-update) | async-done | bytes 5242896 | tf_op jit(solution)/shard_map/all_gather | solution.py:62
  118.1 6.6 %fusion.21 = bf16[1,1,640,512]{3,2,1,0:T(8,128)(2,1)S(1)} fusion(bf16[640,4096]{1,0:T(8,128)(2,1)} %all-gather.6.cloned.1.call-done, bf16[1,4096,512]{2,1,0:T(8,128)(2,1)} %param.15), kind=kOutput, calls=%fused_computation.17 | convolution fusion | flops 2684682240 | bytes 10092544 | tf_op jit(solution)/shard_map/erh,ehd->erd/dot_general | solution.py:63
  124.8 0.0 copy-start.3
  124.8 0.0 copy-start
  124.9 23.4 %all_to_all.15 = bf16[8,1,1,80,512]{4,3,2,1,0:T(8,128)(2,1)S(1)} all-to-all(bf16[8,1,1,80,512]{4,3,2,1,0:T(8,128)(2,1)S(1)} %fusion.32), channel_id=1, replica_groups=mesh['ep'=8,'tp'=4] {'ep'}, dimensions={0} | all-to-all | bytes 1310720 | tf_op jit(solution)/shard_map/all_to_all | solution.py:12
  148.3 0.0 copy-done.3
  148.3 0.6 fusion.18
  148.9 0.1 multiply_reduce_fusion
  149.1 6.0 %psum.15 = f32[256]{0:T(256)S(1)} all-reduce(f32[256]{0:T(256)S(1)} %multiply_reduce_fusion), channel_id=1, replica_groups=mesh['ep'=8,'tp'=4] {'tp'}, use_global_device_ids=true, to_apply=%region_8.9 | all-reduce | flops 256 | bytes 2048 | tf_op jit(solution)/shard_map/psum | solution.py:73
  155.0 0.0 copy-done
  155.0 0.8 multiply_convert_fusion.1
  (13 shorter events, 0.1 us)
Async XLA Ops:
  6.5 61.2 %all-gather.4.cloned.1.call-start = ((), (), s32[]{:S(2)}) async-start(), calls=%async_computation.2 | async-start | bytes 3276800 | tf_op jit(solution)/shard_map/all_gather | solution.py:58
  43.3 74.8 %all-gather.6.cloned.1.call-start = ((), (), s32[]{:S(2)}) async-start(), calls=%async_computation.3 | async-start | bytes 6553600 | tf_op jit(solution)/shard_map/all_gather | solution.py:62
  67.7 5.6 %copy-start.1 = (bf16[1,2048,1024]{2,1,0:T(8,128)(2,1)S(1)}, bf16[1,2048,1024]{2,1,0:T(8,128)(2,1)}, u32[]{:S(2)}) copy-start(bf16[1,2048,1024]{2,1,0:T(8,128)(2,1)} %param.14) | copy-start | bytes 12582916
  67.7 5.6 %copy-start.2 = (bf16[1,640,2048]{2,1,0:T(8,128)(2,1)S(1)}, bf16[1,640,2048]{2,1,0:T(8,128)(2,1)}, u32[]{:S(2)}) copy-start(bf16[1,640,2048]{2,1,0:T(8,128)(2,1)} %all-gather.4.cloned.1.call-done) | copy-start | bytes 7864324
  124.8 23.5 %copy-start.3 = (f32[256,2]{0,1:T(2,128)S(1)}, f32[256,2]{0,1:T(2,128)}, u32[]{:S(2)}) copy-start(f32[256,2]{0,1:T(2,128)} %param.10) | copy-start | bytes 6148
  124.8 30.2 %copy-start = (f32[512]{0:T(512)S(1)}, f32[512]{0:T(512)}, u32[]{:S(2)}) copy-start(f32[512]{0:T(512)} %param.12) | copy-start | bytes 6148
Sparse Core Ops, SparseCore 0:
  43.5 24.2 all-gather.3
  77.7 40.3 all-gather.5
